TPU v7x, 256 devices: a whole 4x4x8 slice. The times are simulated.
256 devices in a mesh: sp: 64 (over z, x, core), tp: 4 (over y).
Axes of the slice: x: 4, y: 4, z: 8, core: 2. Of those that a mesh axis runs over, the one named last changes fastest.
Arguments:
- inputs: bfloat16 [32768, 2048], P('sp', 'tp'), may hold values from -45 to 45
- norm_gain: float32 [3, 2048], replicated, may hold values from 0.1 to 1.9
- w_value: bfloat16 [3, 2048, 1024], P(None, 'sp', 'tp'), may hold values from -0.125 to 0.125
- w_gate: bfloat16 [3, 2048, 1024], P(None, 'sp', 'tp'), may hold values from -0.125 to 0.125
- conv_taps: float32 [3, 31, 1024], P(None, None, 'tp'), may hold values from -5 to 5
- ln_gain: float32 [3, 1024], P(None, 'tp'), may hold values from 0.1 to 1.9
- ln_bias: float32 [3, 1024], P(None, 'tp'), may hold values from -3 to 3
- w_out: bfloat16 [3, 1024, 2048], P(None, 'tp', 'sp'), may hold values from -0.1875 to 0.1875
Outputs:
- stream: bfloat16 [32768, 2048], P('sp', 'tp')
All inputs are finite; a program needn't handle non-finite values.
Results may differ from a plain program's by a relative error of at most 0.01.
Values may be sent and summed in bfloat16 or wider, within the bound.
No kernel may reach another device: no remote copies, remote signals or barrier semaphores. Data moves between devices by JAX's collectives and lax.ppermute only.
A program may use at most 64 MiB of HBM per device.

v0:
```python
import jax
import jax.numpy as jnp
from jax import lax
from jax.sharding import PartitionSpec as P


def turned_gather(arrays, axis, dims):
    turned = [jnp.moveaxis(a, dim, 0) for a, dim in zip(arrays, dims)]
    both = jnp.concatenate([t.reshape(len(t), -1) for t in turned], axis=1)
    out, at, gathered = (lax.all_gather(both, axis, axis=0, tiled=True), 0, [])
    for t, dim in zip(turned, dims):
        piece = out[:, at : at + t[0].size].reshape(-1, *t.shape[1:])
        gathered.append(jnp.moveaxis(piece, 0, dim))
        at += t[0].size
    return tuple(gathered)


def laid_out(blocks, dim):
    blocks = jnp.moveaxis(blocks, 0, dim)
    dims = blocks.shape
    return blocks.reshape(*dims[:dim], dims[dim] * dims[dim + 1], *dims[dim + 2 :])


def copy_for_each(array, axis):
    count = lax.axis_size(axis)
    return lax.all_to_all(
        jnp.broadcast_to(array[None], (count, *array.shape)), axis, 0, 0, tiled=True
    )


def collect(array, axis, dim):
    return laid_out(copy_for_each(array, axis), dim)


def from_behind(block, axis, distance):
    devices = range(lax.axis_size(axis))
    route = [(i - distance, i) for i in devices if i - distance in devices]
    return lax.ppermute(block, axis, route)


def taken_together(array, axis):
    return copy_for_each(array, axis).sum(axis=0)


def packed_total(arrays, axis):
    ends = [0]
    for a in arrays:
        ends.append(ends[-1] + a.size)
    so_far = taken_together(jnp.concatenate([a.ravel() for a in arrays]), axis)
    return tuple((so_far[b:e].reshape(a.shape) for a, b, e in zip(arrays, ends, ends[1:])))


def cut_along(array, dim, count):
    dims = array.shape
    blocks = array.reshape(*dims[:dim], count, dims[dim] // count, *dims[dim + 1 :])
    return jnp.moveaxis(blocks, dim, 0)


def sent_and_summed(array, axis, dim):
    count = lax.axis_size(axis)
    blocks = lax.all_to_all(cut_along(array, dim, count), axis, 0, 0, tiled=True)
    return jnp.sum(blocks.astype(jnp.float32), axis=0)


def shards(inputs, norm_gain, w_value, w_gate, conv_taps, ln_gain, ln_bias, w_out):
    rows = inputs.shape[0]
    reach = conv_taps.shape[1] - 1
    layers = conv_taps.shape[0]
    channels = conv_taps.shape[2] * lax.axis_size("tp")
    whole_value, whole_gate, whole_out = turned_gather((w_value, w_gate, w_out), "sp", (1, 1, 2))
    stream = inputs
    for layer in range(layers):
        full_rows = collect(stream, "tp", 1)
        xf = full_rows.astype(jnp.float32)
        meansq = jnp.mean(xf * xf, axis=1, keepdims=True)
        hidden = (xf * lax.rsqrt(meansq + 1e-06) * norm_gain[layer][None, :]).astype(jnp.bfloat16)
        value = jnp.dot(hidden, whole_value[layer], preferred_element_type=jnp.float32)
        gate = jnp.dot(hidden, whole_gate[layer], preferred_element_type=jnp.float32)
        glu = (value * jax.nn.sigmoid(gate)).astype(jnp.bfloat16)
        rim = from_behind(glu[rows - reach :], "sp", 1)
        padded = jnp.concatenate([rim, glu], axis=0)
        count = padded.shape[0] - reach
        filtered = jnp.zeros((count, glu.shape[1]), jnp.float32)
        for tap in range(reach + 1):
            filtered = filtered + conv_taps[layer, tap][None, :] * padded[tap : tap + count].astype(
                jnp.float32
            )
        total_sum, total_sq = packed_total(
            (jnp.sum(filtered, axis=1), jnp.sum(filtered * filtered, axis=1)), "tp"
        )
        mean_val = (total_sum / channels)[:, None]
        var_val = (total_sq / channels)[:, None] - mean_val * mean_val
        normed = jax.nn.silu(
            (filtered - mean_val) * lax.rsqrt(var_val + 1e-06) * ln_gain[layer][None, :]
            + ln_bias[layer][None, :]
        ).astype(jnp.bfloat16)
        partial_out = jnp.dot(normed, whole_out[layer], preferred_element_type=jnp.float32)
        summed = sent_and_summed(partial_out.astype(jnp.bfloat16), "tp", 1)
        kept = stream.astype(jnp.float32)
        stream = (kept + summed).astype(jnp.bfloat16)
    return stream


def solution(mesh):
    in_specs = (
        P("sp", "tp"),
        P(),
        P(None, "sp", "tp"),
        P(None, "sp", "tp"),
        P(None, None, "tp"),
        P(None, "tp"),
        P(None, "tp"),
        P(None, "tp", "sp"),
    )
    out_specs = P("sp", "tp")
    return jax.shard_map(shards, mesh=mesh, in_specs=in_specs, out_specs=out_specs, check_vma=False)
```

profile of v0, /device:TPU:4, one launch (start us, length us, event | category | flops | bytes accessed | tf_op | source)
XLA Modules:
  0.0 334.8 jit_solution(13739559751142840529)
XLA Ops:
  6.5 0.8 copy.95
  7.3 0.8 copy.94
  8.1 0.8 copy.93
  8.9 0.7 pad_maximum_fusion.3
  9.6 0.0 all-gather.2.cloned.1.call-update
  9.6 1.3 copy.60
  10.9 1.5 broadcast_in_dim.12
  12.4 4.5 %all-to-all-start = ((bf16[4,512,512]{1,2,0:T(8,128)(2,1)}), bf16[4,512,512]{1,2,0:T(8,128)(2,1)S(1)}, u32[]{:S(2)}, u32[]{:S(2)}) async-start(bf16[4,512,512]{1,2,0:T(8,128)(2,1)} %broadcast_in_dim.12), calls=%async_computation | async-start | bytes 4194304 | tf_op jit(solution)/shard_map/all_to_all | solution.py:26
  16.9 0.1 slice_reduce_fusion
  17.0 26.2 %all-to-all-done = bf16[4,512,512]{1,2,0:T(8,128)(2,1)S(1)} async-done(((bf16[4,512,512]{1,2,0:T(8,128)(2,1)}), bf16[4,512,512]{1,2,0:T(8,128)(2,1)S(1)}, u32[]{:S(2)}, u32[]{:S(2)}) %all-to-all-start) | async-done | bytes 2097184 | tf_op jit(solution)/shard_map/all_to_all | solution.py:26
  43.2 0.5 fusion
  43.7 1.9 fusion.2
  45.6 50.0 %all-gather.2.cloned.1.call-done = bf16[2048,2304]{1,0:T(8,128)(2,1)} async-done(((bf16[32,2304]{1,0:T(8,128)(2,1)}), bf16[2048,2304]{1,0:T(8,128)(2,1)}) %all-gather.2.cloned.1.call-update) | async-done | bytes 9437200 | tf_op jit(solution)/shard_map/all_gather | solution.py:10
  95.6 6.1 %fusion.129 = (bf16[2048,768]{1,0:T(8,128)(2,1)}, bf16[2048,768]{1,0:T(8,128)(2,1)S(1)}, bf16[2048,768]{1,0:T(8,128)(2,1)}) fusion(bf16[2048,2304]{1,0:T(8,128)(2,1)} %all-gather.2.cloned.1.call-done), kind=kLoop, calls=%fused_computation.292 | loop fusion | bytes 18874368 | tf_op jit(solution)/shard_map/slice | solution.py:12
  101.6 4.8 %copy.66 = bf16[2048,768]{0,1:T(8,128)(2,1)} copy(bf16[2048,768]{1,0:T(8,128)(2,1)} %get-tuple-element.19) | data formatting | bytes 6291456 | tf_op jit(solution)/shard_map/slice | solution.py:12
  106.4 4.7 %copy.64 = bf16[2048,768]{0,1:T(8,128)(2,1)} copy(bf16[2048,768]{1,0:T(8,128)(2,1)} %get-tuple-element.17) | data formatting | bytes 6291456 | tf_op jit(solution)/shard_map/slice | solution.py:12
  111.1 2.8 fusion.17
  113.9 2.0 fusion.18
  115.9 2.2 collective-permute-start
  118.1 2.9 collective-permute-done
  121.0 3.0 fusion.128
  124.0 0.6 broadcast_in_dim.13
  124.6 4.3 %all-to-all-start.1 = ((f32[4,1,1024]{2,1,0:T(1,128)}), f32[4,1,1024]{2,1,0:T(1,128)S(1)}, u32[]{:S(2)}, u32[]{:S(2)}) async-start(f32[4,1,1024]{2,1,0:T(1,128)} %broadcast_in_dim.13), calls=%async_computation.1 | async-start | bytes 32768 | tf_op jit(solution)/shard_map/all_to_all | solution.py:26
  128.9 3.0 copy.69
  131.9 2.4 all-to-all-done.1
  134.3 2.2 convolution_convert_fusion.2
  136.5 0.2 copy.101
  136.7 27.0 %all_to_all.48 = bf16[4,512,512]{2,1,0:T(8,128)(2,1)S(1)} all-to-all(bf16[4,512,512]{2,1,0:T(8,128)(2,1)S(1)} %bitcast.186), channel_id=1, replica_groups=mesh['sp'=64,'tp'=4] {'tp'}, dimensions={0} | all-to-all | bytes 4194304 | tf_op jit(solution)/shard_map/all_to_all | solution.py:61
  163.7 0.3 convert_reduce_fusion.2
  164.0 0.2 add_convert_fusion.2
  164.2 0.2 copy.71
  164.4 1.5 broadcast_in_dim.14
  165.9 3.6 %all-to-all-start.3 = ((bf16[4,512,512]{1,2,0:T(8,128)(2,1)}), bf16[4,512,512]{1,2,0:T(8,128)(2,1)S(1)}, u32[]{:S(2)}, u32[]{:S(2)}) async-start(bf16[4,512,512]{1,2,0:T(8,128)(2,1)} %broadcast_in_dim.14), calls=%async_computation.3 | async-start | bytes 4194304 | tf_op jit(solution)/shard_map/all_to_all | solution.py:26
  169.6 23.2 %all-to-all-done.3 = bf16[4,512,512]{1,2,0:T(8,128)(2,1)S(1)} async-done(((bf16[4,512,512]{1,2,0:T(8,128)(2,1)}), bf16[4,512,512]{1,2,0:T(8,128)(2,1)S(1)}, u32[]{:S(2)}, u32[]{:S(2)}) %all-to-all-start.3) | async-done | bytes 2097184 | tf_op jit(solution)/shard_map/all_to_all | solution.py:26
  192.7 0.5 fusion.3
  193.2 0.5 fusion.5
  193.8 2.0 fusion.14
  195.8 2.0 fusion.19
  197.8 2.1 collective-permute-start.1
  200.0 2.9 collective-permute-done.1
  202.9 2.4 fusion.127
  205.4 7.7 %all_to_all.49 = f32[4,1,1024]{2,1,0:T(1,128)S(1)} all-to-all(f32[4,1,1024]{2,1,0:T(1,128)S(1)} %broadcast_in_dim.15), channel_id=1, replica_groups=mesh['sp'=64,'tp'=4] {'tp'}, dimensions={0} | all-to-all | bytes 32768 | tf_op jit(solution)/shard_map/all_to_all | solution.py:26
  213.1 2.0 convolution_convert_fusion.1
  215.1 0.2 copy.100
  215.3 29.3 %all_to_all.50 = bf16[4,512,512]{2,1,0:T(8,128)(2,1)S(1)} all-to-all(bf16[4,512,512]{2,1,0:T(8,128)(2,1)S(1)} %bitcast.187), channel_id=1, replica_groups=mesh['sp'=64,'tp'=4] {'tp'}, dimensions={0} | all-to-all | bytes 4194304 | tf_op jit(solution)/shard_map/all_to_all | solution.py:61
  244.7 0.3 convert_reduce_fusion.1
  245.0 0.2 add_convert_fusion.1
  245.2 0.2 copy.76
  245.4 1.5 broadcast_in_dim.16
  246.9 3.6 %all-to-all-start.6 = ((bf16[4,512,512]{1,2,0:T(8,128)(2,1)}), bf16[4,512,512]{1,2,0:T(8,128)(2,1)S(1)}, u32[]{:S(2)}, u32[]{:S(2)}) async-start(bf16[4,512,512]{1,2,0:T(8,128)(2,1)} %broadcast_in_dim.16), calls=%async_computation.6 | async-start | bytes 4194304 | tf_op jit(solution)/shard_map/all_to_all | solution.py:26
  250.5 27.4 %all-to-all-done.6 = bf16[4,512,512]{1,2,0:T(8,128)(2,1)S(1)} async-done(((bf16[4,512,512]{1,2,0:T(8,128)(2,1)}), bf16[4,512,512]{1,2,0:T(8,128)(2,1)S(1)}, u32[]{:S(2)}, u32[]{:S(2)}) %all-to-all-start.6) | async-done | bytes 2097184 | tf_op jit(solution)/shard_map/all_to_all | solution.py:26
  277.9 0.5 fusion.6
  278.4 0.5 fusion.8
  279.0 2.0 fusion.11
  281.0 2.0 fusion.20
  283.0 1.9 collective-permute-start.2
  285.0 3.1 collective-permute-done.2
  288.1 2.4 fusion.126
  290.5 7.7 %all_to_all.51 = f32[4,1,1024]{2,1,0:T(1,128)S(1)} all-to-all(f32[4,1,1024]{2,1,0:T(1,128)S(1)} %broadcast_in_dim.17), channel_id=1, replica_groups=mesh['sp'=64,'tp'=4] {'tp'}, dimensions={0} | all-to-all | bytes 32768 | tf_op jit(solution)/shard_map/all_to_all | solution.py:26
  298.3 2.0 convolution_convert_fusion
  300.3 0.2 copy.99
  300.5 26.1 %all_to_all.52 = bf16[4,512,512]{2,1,0:T(8,128)(2,1)S(1)} all-to-all(bf16[4,512,512]{2,1,0:T(8,128)(2,1)S(1)} %bitcast.188), channel_id=1, replica_groups=mesh['sp'=64,'tp'=4] {'tp'}, dimensions={0} | all-to-all | bytes 4194304 | tf_op jit(solution)/shard_map/all_to_all | solution.py:61
  326.7 0.3 convert_reduce_fusion
  327.0 1.0 add_convert_fusion
  (40 shorter events, 0.4 us)
Async XLA Ops:
  6.5 89.0 %all-gather.2.cloned.1.call-start = ((), (), s32[]{:S(2)}) async-start(), calls=%async_computation.9 | async-start | bytes 9584640 | tf_op jit(solution)/shard_map/all_gather | solution.py:10
  10.9 6.0 %copy-start.3 = (f32[3,2048]{1,0:T(4,128)S(1)}, f32[3,2048]{1,0:T(4,128)}, u32[]{:S(2)}) copy-start(f32[3,2048]{1,0:T(4,128)} %param.9) | copy-start | bytes 73732
  10.9 6.0 %copy-start.2 = (f32[3,31,256]{2,1,0:T(8,128)S(1)}, f32[3,31,256]{2,1,0:T(8,128)}, u32[]{:S(2)}) copy-start(f32[3,31,256]{2,1,0:T(8,128)} %param.12) | copy-start | bytes 285700
  12.4 30.8 %all-to-all-start = ((bf16[4,512,512]{1,2,0:T(8,128)(2,1)}), bf16[4,512,512]{1,2,0:T(8,128)(2,1)S(1)}, u32[]{:S(2)}, u32[]{:S(2)}) async-start(bf16[4,512,512]{1,2,0:T(8,128)(2,1)} %broadcast_in_dim.12), calls=%async_computation | async-start | bytes 4194304 | tf_op jit(solution)/shard_map/all_to_all | solution.py:26
  111.1 2.8 copy-start
  113.9 4.2 %copy-start.4 = (f32[3,256]{1,0:T(4,128)S(1)}, f32[3,256]{1,0:T(4,128)}, u32[]{:S(2)}) copy-start(f32[3,256]{1,0:T(4,128)} %param.14) | copy-start | bytes 9220
  113.9 15.0 %copy-start.5 = (f32[3,256]{1,0:T(4,128)S(1)}, f32[3,256]{1,0:T(4,128)}, u32[]{:S(2)}) copy-start(f32[3,256]{1,0:T(4,128)} %param.13) | copy-start | bytes 9220
  115.9 5.1 %collective-permute-start = (bf16[30,256]{1,0:T(8,128)(2,1)S(1)}, bf16[30,256]{1,0:T(8,128)(2,1)S(1)}, u32[]{:S(2)}, u32[]{:S(2)}) collective-permute-start(bf16[30,256]{1,0:T(8,128)(2,1)S(1)} %slice.856), channel_id=1, source_target_pairs={{0,4},{4,8},{8,12},{12,16},{16,20},{20,24},{24,28},{28,32},{32,36}... | collective-permute-start | bytes 46088 | tf_op jit(solution)/shard_map/ppermute | solution.py:38
  124.6 9.6 %all-to-all-start.1 = ((f32[4,1,1024]{2,1,0:T(1,128)}), f32[4,1,1024]{2,1,0:T(1,128)S(1)}, u32[]{:S(2)}, u32[]{:S(2)}) async-start(f32[4,1,1024]{2,1,0:T(1,128)} %broadcast_in_dim.13), calls=%async_computation.1 | async-start | bytes 32768 | tf_op jit(solution)/shard_map/all_to_all | solution.py:26
  136.7 27.3 %copy-start.1 = (bf16[512,512]{1,0:T(8,128)(2,1)S(1)}, bf16[512,512]{1,0:T(8,128)(2,1)}, u32[]{:S(2)}) copy-start(bf16[512,512]{1,0:T(8,128)(2,1)} %param.8) | copy-start | bytes 1572868
  165.9 26.8 %all-to-all-start.3 = ((bf16[4,512,512]{1,2,0:T(8,128)(2,1)}), bf16[4,512,512]{1,2,0:T(8,128)(2,1)S(1)}, u32[]{:S(2)}, u32[]{:S(2)}) async-start(bf16[4,512,512]{1,2,0:T(8,128)(2,1)} %broadcast_in_dim.14), calls=%async_computation.3 | async-start | bytes 4194304 | tf_op jit(solution)/shard_map/all_to_all | solution.py:26
  197.8 5.1 %collective-permute-start.1 = (bf16[30,256]{1,0:T(8,128)(2,1)S(1)}, bf16[30,256]{1,0:T(8,128)(2,1)S(1)}, u32[]{:S(2)}, u32[]{:S(2)}) collective-permute-start(bf16[30,256]{1,0:T(8,128)(2,1)S(1)} %slice.919), channel_id=1, source_target_pairs={{0,4},{4,8},{8,12},{12,16},{16,20},{20,24},{24,28},{28,32},{32,36}... | collective-permute-start | bytes 46088 | tf_op jit(solution)/shard_map/ppermute | solution.py:38
  246.9 31.1 %all-to-all-start.6 = ((bf16[4,512,512]{1,2,0:T(8,128)(2,1)}), bf16[4,512,512]{1,2,0:T(8,128)(2,1)S(1)}, u32[]{:S(2)}, u32[]{:S(2)}) async-start(bf16[4,512,512]{1,2,0:T(8,128)(2,1)} %broadcast_in_dim.16), calls=%async_computation.6 | async-start | bytes 4194304 | tf_op jit(solution)/shard_map/all_to_all | solution.py:26
  283.0 5.1 %collective-permute-start.2 = (bf16[30,256]{1,0:T(8,128)(2,1)S(1)}, bf16[30,256]{1,0:T(8,128)(2,1)S(1)}, u32[]{:S(2)}, u32[]{:S(2)}) collective-permute-start(bf16[30,256]{1,0:T(8,128)(2,1)S(1)} %slice.981), channel_id=1, source_target_pairs={{0,4},{4,8},{8,12},{12,16},{16,20},{20,24},{24,28},{28,32},{32,36}... | collective-permute-start | bytes 46088 | tf_op jit(solution)/shard_map/ppermute | solution.py:38
Sparse Core Ops, SparseCore 0:
  10.1 85.4 all-gather.1
where the time goes:
time: 336 us; the launch traced here: 335 us
  waiting for transfers between devices  138 us (41%)
  blocking collectives  97.9 us (29%)
  local copies, waits for them, and re-layouts  28.5 us (8%)
  starting transfers between devices  22.1 us (7%)
  matrix products  19.1 us (6%)
  other arithmetic  15.3 us (5%)
  between operations  13.8 us (4%)
    all_to_all x3, blocking collectives, sent_and_summed(): lax.all_to_all(cut_along(array, dim, count), axis, 0, 0, tiled=True)  82.5 us
    all_to_all x4, waiting for transfers between devices, copy_for_each(): lax.all_to_all(jnp.broadcast_to(array[None], (count, *array.shape)), axis...  79.2 us
    all_gather x1, waiting for transfers between devices, turned_gather(): out, at, gathered = (lax.all_gather(both, axis, axis=0, tiled=True), 0, [])  50 us
    slice x4, local copies, waits for them, and re-layouts, turned_gather(): piece = out[:, at:at + t[0].size].reshape(-1, *t.shape[1:])  18.5 us
    all_to_all x4, starting transfers between devices, copy_for_each(): lax.all_to_all(jnp.broadcast_to(array[None], (count, *array.shape)), axis...  16 us
    all_to_all x2, blocking collectives, copy_for_each(): lax.all_to_all(jnp.broadcast_to(array[None], (count, *array.shape)), axis...  15.4 us
    ppermute x3, waiting for transfers between devices, from_behind(): return lax.ppermute(block, axis, route)  8.89 us
    reduce_sum x3, other arithmetic, shards(): jnp.sum(filtered, axis=1)  7.83 us
  transfers between devices with their start and end apart: 8, of which 8 were waited for; matrix products, arithmetic and copies ran while one was open for 2% of the time, Pallas kernels for 0%

commit v1 on v0

v1 whole, which is shorter than its diff:
```python
import functools

import jax
import jax.numpy as jnp
from jax import lax
from jax.experimental import pallas as pl
from jax.experimental.pallas import tpu as pltpu
from jax.sharding import PartitionSpec as P

HALO = 32
ROWS = 32


def module_kernel(
    reach, first_ref, x_ref, gain_ref, wv_ref, wg_ref, wo_ref, taps_ref, lng_ref, lnb_ref,
    out_ref, hid_ref, glu_ref, fil_ref, norm_ref,
):
    step = pl.program_id(0)
    parts, rows_in, width = x_ref.shape
    rows = rows_in - HALO
    wide = glu_ref.shape[1]
    blocks = fil_ref.shape[0]

    @pl.when(step == 0)
    def _():
        total = jnp.zeros((rows_in, 1), jnp.float32)
        for q in range(parts):
            xf = x_ref[q].astype(jnp.float32)
            total = total + jnp.sum(xf * xf, axis=1, keepdims=True)
        scale = lax.rsqrt(total / (parts * width) + 1e-06)
        for q in range(parts):
            cols = slice(q * width, (q + 1) * width)
            xf = x_ref[q].astype(jnp.float32)
            hid_ref[:, cols] = (xf * scale * gain_ref[:, cols]).astype(jnp.bfloat16)

    @pl.when(step < blocks)
    def _():
        hidden = hid_ref[...]
        depth = hidden.shape[1]
        value = jnp.dot(hidden, wv_ref[...].reshape(depth, wide), preferred_element_type=jnp.float32)
        gate = jnp.dot(hidden, wg_ref[...].reshape(depth, wide), preferred_element_type=jnp.float32)
        glu = (value * jax.nn.sigmoid(gate)).astype(jnp.bfloat16).astype(jnp.float32)
        row = lax.broadcasted_iota(jnp.int32, (rows_in, 1), 0)
        glu_ref[...] = jnp.where(row < first_ref[0], 0.0, glu)
        lead = HALO - reach
        for r in range(0, rows, ROWS):
            acc = jnp.zeros((ROWS, wide), jnp.float32)
            for tap in range(reach + 1):
                acc = acc + taps_ref[0, tap : tap + 1, :] * glu_ref[pl.ds(r + lead + tap, ROWS), :]
            fil_ref[step, pl.ds(r, ROWS), :] = acc

    @pl.when(step == blocks)
    def _():
        channels = blocks * wide
        total = jnp.zeros((rows, 1), jnp.float32)
        square = jnp.zeros((rows, 1), jnp.float32)
        for b in range(blocks):
            f = fil_ref[b]
            total = total + jnp.sum(f, axis=1, keepdims=True)
            square = square + jnp.sum(f * f, axis=1, keepdims=True)
        mean = total / channels
        scale = lax.rsqrt(square / channels - mean * mean + 1e-06)
        for b in range(blocks):
            cols = slice(b * wide, (b + 1) * wide)
            v = (fil_ref[b] - mean) * scale * lng_ref[:, cols] + lnb_ref[:, cols]
            norm_ref[:, cols] = (v * jax.nn.sigmoid(v)).astype(jnp.bfloat16)

    @pl.when(step >= blocks)
    def _():
        acc = jnp.zeros((rows, width), jnp.float32)
        for b in range(blocks):
            acc = acc + lax.dot_general(
                norm_ref[:, b * wide : (b + 1) * wide],
                wo_ref[b].reshape(width, wide),
                (((1,), (1,)), ((), ())),
                preferred_element_type=jnp.float32,
            )
        kept = x_ref[step - blocks, HALO:, :].astype(jnp.float32)
        out_ref[0] = (kept + acc).astype(jnp.bfloat16)


def module(first, x, gain, weights, layer, taps, ln_gain, ln_bias):
    parts, rows_in, width = x.shape
    rows = rows_in - HALO
    blocks, shards, kinds, depth, wide = weights.shape
    reach = taps.shape[0] - 1
    taps = taps.reshape(reach + 1, blocks, wide).transpose(1, 0, 2)
    kind = 3 * layer
    group = shards // parts
    ahead = lambda i: jnp.minimum(i, blocks - 1)
    after = lambda i: jnp.maximum(i - blocks, 0)
    whole = lambda *shape: pl.BlockSpec(shape, lambda i: (0,) * len(shape))
    return pl.pallas_call(
        functools.partial(module_kernel, reach),
        grid=(blocks + parts,),
        in_specs=[
            pl.BlockSpec(memory_space=pltpu.SMEM),
            whole(parts, rows_in, width),
            whole(1, parts * width),
            pl.BlockSpec((None, shards, None, depth, wide), lambda i: (ahead(i), 0, kind, 0, 0)),
            pl.BlockSpec((None, shards, None, depth, wide), lambda i: (ahead(i), 0, kind + 1, 0, 0)),
            pl.BlockSpec((blocks, group, None, depth, wide), lambda i: (0, after(i), kind + 2, 0, 0)),
            pl.BlockSpec((1, reach + 1, wide), lambda i: (ahead(i), 0, 0)),
            whole(1, blocks * wide),
            whole(1, blocks * wide),
        ],
        out_specs=pl.BlockSpec((1, rows, width), lambda i: (after(i), 0, 0)),
        out_shape=jax.ShapeDtypeStruct((parts, rows, width), jnp.bfloat16),
        scratch_shapes=[
            pltpu.VMEM((rows_in, parts * width), jnp.bfloat16),
            pltpu.VMEM((rows_in, wide), jnp.float32),
            pltpu.VMEM((blocks, rows, wide), jnp.float32),
            pltpu.VMEM((rows, blocks * wide), jnp.bfloat16),
        ],
        compiler_params=pltpu.CompilerParams(dimension_semantics=("arbitrary",)),
        name=f"module_{layer}",
    )(first, x, gain[None], weights, weights, weights, taps, ln_gain[None], ln_bias[None])


def shards(inputs, norm_gain, w_value, w_gate, conv_taps, ln_gain, ln_bias, w_out):
    layers = norm_gain.shape[0]
    sp, tp = lax.axis_size("sp"), lax.axis_size("tp")
    rows = inputs.shape[0] // tp
    lead = layers * HALO
    kinds = jnp.stack((w_value, w_gate, jnp.swapaxes(w_out, 1, 2)), axis=1)
    depth, wide = kinds.shape[2:]
    packed = kinds.reshape(-1, wide)
    weights = lax.all_gather(packed, ("tp", "sp"), axis=0, tiled=True)
    weights = weights.reshape(tp, sp, 3 * layers, depth, wide)
    before = lax.ppermute(inputs[-lead:], "sp", [(i, i + 1) for i in range(sp - 1)])
    padded = jnp.concatenate((before, inputs), axis=0)
    windows = jnp.stack([padded[k * rows : (k + 1) * rows + lead] for k in range(tp)])
    x = lax.all_to_all(windows, "tp", 0, 0, tiled=True)
    start = (lax.axis_index("sp") * tp + lax.axis_index("tp")) * rows
    small = lax.all_gather(
        jnp.concatenate((conv_taps, ln_gain[:, None], ln_bias[:, None]), axis=1), "tp", axis=2, tiled=True
    )
    for layer in range(layers):
        first = jnp.maximum((layers - layer) * HALO - start, 0).astype(jnp.int32)[None]
        x = module(
            first, x, norm_gain[layer], weights, layer,
            small[layer, :-2], small[layer, -2], small[layer, -1],
        )
    return lax.all_to_all(x, "tp", 0, 0, tiled=True).reshape(inputs.shape)


def solution(mesh):
    in_specs = (
        P("sp", "tp"),
        P(),
        P(None, "sp", "tp"),
        P(None, "sp", "tp"),
        P(None, None, "tp"),
        P(None, "tp"),
        P(None, "tp"),
        P(None, "tp", "sp"),
    )
    out_specs = P("sp", "tp")
    return jax.shard_map(shards, mesh=mesh, in_specs=in_specs, out_specs=out_specs, check_vma=False)
```

time: 336 us -> 235 us (0.70)
  blocking collectives: 97.9 us -> 27.4 us
  Pallas kernels: 0 us -> 39.1 us
  local copies, waits for them, and re-layouts: 28.5 us -> 7.42 us
  matrix products: 19.1 us -> 0 us
  starting transfers between devices: 22.1 us -> 5.68 us
  other arithmetic: 15.3 us -> 4.78 us
    all_to_all x5 -> x1, blocking collectives: 97.9 us -> 13.6 us  [shards(): return lax.all_to_all(x, 'tp', 0, 0, tiled=True).reshape(inputs.shape)]
    all_gather x1, waiting for transfers between devices: 50 us -> 126 us  [shards(): weights = lax.all_gather(packed, ('tp', 'sp'), axis=0, tiled=True)]
    all_to_all x4 -> x1, waiting for transfers between devices: 79.2 us -> 9.76 us  [shards(): x = lax.all_to_all(windows, 'tp', 0, 0, tiled=True)]
    pallas_call x0 -> x3, Pallas kernels: none -> 39.1 us  [module(): pl.pallas_call(functools.partial(module_kernel, reach), grid=(blocks + pa...]
    dot_general x9 -> x0, matrix products: 19.1 us -> none  [the longest x3 6.82 us: shards(): jnp.dot(hidden, whole_gate[layer], preferred_element_type=jnp.float32)]
    slice x15 -> x3, local copies, waits for them, and re-layouts: 18.7 us -> 2.41 us  [the longest x1 1.49 us: shards(): norm_gain[layer]]
    all_gather x0 -> x1, blocking collectives: none -> 13.8 us  [shards(): lax.all_gather(jnp.concatenate((conv_taps, ln_gain[:, None], ln_bias[:, N...]
    all_to_all x4 -> x1, starting transfers between devices: 16 us -> 3.77 us  [shards(): x = lax.all_to_all(windows, 'tp', 0, 0, tiled=True)]
  transfers between devices with their start and end apart: 8 -> 3, of which waited for: 8 -> 2; matrix products, arithmetic and copies ran while one was open for 2% -> 4% of each run, Pallas kernels for 0% -> 0%
where the time goes in v1:
time: 235 us; the launch traced here: 233 us
  waiting for transfers between devices  136 us (58%)
  Pallas kernels  39.1 us (17%)
  blocking collectives  27.4 us (12%)
  between operations  13.4 us (6%)
  local copies, waits for them, and re-layouts  7.42 us (3%)
  starting transfers between devices  5.68 us (2%)
  other arithmetic  4.78 us (2%)
    all_gather x1, waiting for transfers between devices, shards(): weights = lax.all_gather(packed, ('tp', 'sp'), axis=0, tiled=True)  126 us
    pallas_call x3, Pallas kernels, module(): pl.pallas_call(functools.partial(module_kernel, reach), grid=(blocks + pa...  39.1 us
    all_gather x1, blocking collectives, shards(): lax.all_gather(jnp.concatenate((conv_taps, ln_gain[:, None], ln_bias[:, N...  13.8 us
    all_to_all x1, blocking collectives, shards(): return lax.all_to_all(x, 'tp', 0, 0, tiled=True).reshape(inputs.shape)  13.6 us
    all_to_all x1, waiting for transfers between devices, shards(): x = lax.all_to_all(windows, 'tp', 0, 0, tiled=True)  9.76 us
  transfers between devices with their start and end apart: 3, of which 2 were waited for; matrix products, arithmetic and copies ran while one was open for 4% of the time, Pallas kernels for 0%

profile of v1, /device:TPU:4, one launch (start us, length us, event | category | flops | bytes accessed | tf_op | source)
XLA Modules:
  0.0 233.4 jit_solution(9172430590230759758)
XLA Ops:
  6.5 0.0 all-gather.2.cloned.1.call-start
  6.5 1.5 pad_maximum_fusion.2
  8.1 0.0 all-gather.2.cloned.1.call-update
  8.1 0.9 slice.51
  9.0 1.9 collective-permute-start
  10.9 0.7 copy.11
  11.6 0.7 copy.12
  12.3 0.9 pad_maximum_fusion.3
  13.2 13.8 %all_gather.7 = f32[3,33,1024]{2,1,0:T(8,128)S(1)} all-gather(f32[3,33,256]{2,1,0:T(8,128)S(1)} %pad_maximum_fusion.3), channel_id=1, replica_groups=mesh['sp'=64,'tp'=4] {'tp'}, dimensions={2}, use_global_device_ids=true | all-gather | bytes 506880 | tf_op jit(solution)/shard_map/all_gather | solution.py:135
  27.0 0.0 collective-permute-done
  27.0 1.3 fusion
  28.3 1.0 pad_maximum_fusion
  29.4 3.8 %all-to-all-start = ((bf16[4,224,512]{2,1,0:T(8,128)(2,1)}), bf16[4,224,512]{2,1,0:T(8,128)(2,1)S(1)}, u32[]{:S(2)}, u32[]{:S(2)}) async-start(bf16[4,224,512]{2,1,0:T(8,128)(2,1)} %pad_maximum_fusion), calls=%async_computation | async-start | bytes 1835008 | tf_op jit(solution)/shard_map/all_to_all | solution.py:133
  33.2 0.1 reshape_squeeze.9
  33.2 0.7 copy.21
  33.9 0.1 reshape_squeeze.10
  34.0 0.7 copy.20
  34.7 0.1 reshape_squeeze.11
  34.7 0.7 copy.19
  35.4 0.6 slice_bitcast_fusion.3
  36.0 1.5 fusion.2
  37.5 9.8 %all-to-all-done.x_ref = bf16[4,224,512]{2,1,0:T(8,128)(2,1)S(1)} async-done(((bf16[4,224,512]{2,1,0:T(8,128)(2,1)}), bf16[4,224,512]{2,1,0:T(8,128)(2,1)S(1)}, u32[]{:S(2)}, u32[]{:S(2)}) %all-to-all-start) | async-done | bytes 917536 | tf_op jit(solution)/shard_map/all_to_all | solution.py:133
  47.3 0.0 copy-start
  47.3 125.8 %all-gather.2.cloned.1.call-done = bf16[73728,256]{1,0:T(8,128)(2,1)} async-done(((bf16[288,256]{1,0:T(8,128)(2,1)}), bf16[73728,256]{1,0:T(8,128)(2,1)}) %all-gather.2.cloned.1.call-update) | async-done | bytes 37748752 | tf_op jit(solution)/shard_map/all_gather | solution.py:128
  173.1 0.0 copy-done
  173.1 14.0 %module_0.1.x_ref = bf16[4,192,512]{2,1,0:T(8,128)(2,1)} custom-call(s32[1]{0:T(128)} %bitcast.2.first_ref, bf16[4,224,512]{2,1,0:T(8,128)(2,1)} %copy-done, f32[1,2048]{1,0:T(1,128)} %get-tuple-element.19.gain_ref, bf16[4,64,9,32,256]{4,3,2,1,0:T(8,128)(2,1)} %bitcast.42, bf16[4,64,9,32,256]{4,3,2,1,0:T(8,128)(2,1)} %bitcast.43, ...), custom_call_target="tpu_custom_call" | custom-call | tf_op jit(solution)/shard_map/module_0/pallas_call | solution.py:93
  187.1 13.0 %module_1.1.x_ref = bf16[4,160,512]{2,1,0:T(8,128)(2,1)} custom-call(s32[1]{0:T(128)} %bitcast.1.first_ref, bf16[4,192,512]{2,1,0:T(8,128)(2,1)} %module_0.1.x_ref, f32[1,2048]{1,0:T(1,128)} %get-tuple-element.20.gain_ref, bf16[4,64,9,32,256]{4,3,2,1,0:T(8,128)(2,1)} %bitcast.45, bf16[4,64,9,32,256]{4,3,2,1,0:T(8,128)(2,1)} %bitcast.46, ...), custom_call_target="tpu_custom_call" | custom-call | tf_op jit(solution)/shard_map/module_1/pallas_call | solution.py:93
  200.0 12.1 %module_2.1 = bf16[4,128,512]{2,1,0:T(8,128)(2,1)} custom-call(s32[1]{0:T(128)} %bitcast.first_ref, bf16[4,160,512]{2,1,0:T(8,128)(2,1)} %module_1.1.x_ref, f32[1,2048]{1,0:T(1,128)} %get-tuple-element.18.gain_ref, bf16[4,64,9,32,256]{4,3,2,1,0:T(8,128)(2,1)} %bitcast.48, bf16[4,64,9,32,256]{4,3,2,1,0:T(8,128)(2,1)} %bitcast.49, ...), custom_call_target="tpu_custom_call" | custom-call | tf_op jit(solution)/shard_map/module_2/pallas_call | solution.py:93
  212.1 13.6 %all_to_all.10 = bf16[4,128,512]{2,1,0:T(8,128)(2,1)S(1)} all-to-all(bf16[4,128,512]{2,1,0:T(8,128)(2,1)} %module_2.1), channel_id=1, replica_groups=mesh['sp'=64,'tp'=4] {'tp'}, dimensions={0} | all-to-all | bytes 1048576 | tf_op jit(solution)/shard_map/all_to_all | solution.py:144
  225.7 0.8 copy.23
  (1 shorter events, 0.0 us)
Async XLA Ops:
  6.5 166.5 %all-gather.2.cloned.1.call-start = ((), (), s32[]{:S(2)}) async-start(), calls=%async_computation.2 | async-start | bytes 37896192 | tf_op jit(solution)/shard_map/all_gather | solution.py:128
  9.0 18.0 %collective-permute-start = (bf16[96,512]{1,0:T(8,128)(2,1)S(1)}, bf16[96,512]{1,0:T(8,128)(2,1)S(1)}, u32[]{:S(2)}, u32[]{:S(2)}) collective-permute-start(bf16[96,512]{1,0:T(8,128)(2,1)S(1)} %slice.51), channel_id=1, source_target_pairs={{0,4},{4,8},{8,12},{12,16},{16,20},{20,24},{24,28},{28,32},{32,36}... | collective-permute-start | bytes 294920 | tf_op jit(solution)/shard_map/ppermute | solution.py:130
  29.4 17.9 %all-to-all-start = ((bf16[4,224,512]{2,1,0:T(8,128)(2,1)}), bf16[4,224,512]{2,1,0:T(8,128)(2,1)S(1)}, u32[]{:S(2)}, u32[]{:S(2)}) async-start(bf16[4,224,512]{2,1,0:T(8,128)(2,1)} %pad_maximum_fusion), calls=%async_computation | async-start | bytes 1835008 | tf_op jit(solution)/shard_map/all_to_all | solution.py:133
  47.3 125.8 %copy-start = (bf16[4,224,512]{2,1,0:T(8,128)(2,1)}, bf16[4,224,512]{2,1,0:T(8,128)(2,1)S(1)}, u32[]{:S(2)}) copy-start(bf16[4,224,512]{2,1,0:T(8,128)(2,1)S(1)} %all-to-all-done.x_ref) | copy-start | bytes 2752516
Sparse Core Ops, SparseCore 0:
  11.1 161.9 all-gather.1
